TPU v7x, 512 devices: a whole 4x4x16 slice. The times are simulated.
512 devices in a mesh: sp: 32 (over z, core), tp: 16 (over y, x).
Axes of the slice: x: 4, y: 4, z: 16, core: 2. Of those that a mesh axis runs over, the one named last changes fastest.
Arguments:
- query_rows: bfloat16 [16384, 1024], P('sp', 'tp'), may hold values from -128 to 128
- key_rows: bfloat16 [16384, 1024], P('sp', 'tp'), may hold values from -4 to 4
- value_rows: bfloat16 [16384, 1024], P('sp', 'tp'), may hold values from -6 to 6
- cum_gates: float32 [16384, 16], P('sp', 'tp'), may hold values from -16386 to 0, as said below
- residual: bfloat16 [16384, 2048], P('sp', 'tp'), may hold values from -64 to 64
- output_weight: bfloat16 [1024, 2048], P(None, 'tp'), may hold values from -0.1875 to 0.1875
- norm_gain: bfloat16 [2048], replicated, may hold values from 0.099609375 to 1.8984375
- expert_index: int32 [16384, 2], P('sp'), may hold values from 0 to 31, all different within a row; in each aligned block of 512 rows (0 to 511, 512 to 1023, ...) at most 64 rows name the same one
- route_weights: float32 [16384, 2], P('sp'), may hold values from 0.2 to 1
- gate_weight: bfloat16 [32, 2048, 2048], P('sp', None, 'tp'), may hold values from -2 to 2
- up_weight: bfloat16 [32, 2048, 2048], P('sp', None, 'tp'), may hold values from -2 to 2
- down_weight: bfloat16 [32, 2048, 2048], P('sp', None, 'tp'), may hold values from -0.125 to 0.125
Outputs:
- layer_out: bfloat16 [16384, 2048], P('sp', 'tp')
Inputs may be any that keep to these rules, and one draw needn't show every extreme that they name: `cum_gates`: each head's values never rise along positions. `expert_index`: each token names 2 different experts. In the 512 tokens of one index of sp no expert is named more than 64 times, and in some index's tokens some expert is named exactly 64 times.
All inputs are finite; a program needn't handle non-finite values.
Results may differ from a plain program's by a relative error of at most 0.01.
Values may be sent and summed in bfloat16 or wider, within the bound.
A program may use at most 64 MiB of HBM per device.

v0:
```python
import math
import jax
import jax.numpy as jnp
from jax import lax
from jax.sharding import PartitionSpec as P

NORM_EPS = 1e-06
CLAMP_LIMIT = 7.0
SILU_ALPHA = 1.702


def joined_along(parts, dim):
    lengths = list(parts.shape[1:])
    lengths[dim] *= parts.shape[0]
    return jnp.moveaxis(parts, 0, dim).reshape(lengths)


def copy_for_each(x, axis):
    copies = jnp.broadcast_to(x, (lax.axis_size(axis), *x.shape))
    return lax.all_to_all(copies, axis, split_axis=0, concat_axis=0, tiled=True)


def gathered_copies(x, axis, dim):
    return joined_along(copy_for_each(x, axis), dim)


def side_by_side(arrays, axis, dim, along):
    widths = [a.shape[along] for a in arrays]
    both = jnp.concatenate(arrays, axis=along)
    result = lax.all_gather(both, axis, axis=dim, tiled=True)
    return tuple(jnp.split(result, [sum(widths[:k]) for k in range(1, len(widths))], axis=along))


def normalize(rows, norm_gain):
    wide = rows.astype(jnp.float32)
    factor = lax.rsqrt(jnp.mean(wide * wide, axis=-1, keepdims=True) + NORM_EPS)
    return (wide * factor * norm_gain.astype(jnp.float32)).astype(jnp.bfloat16)


def attend_local(query_rows, key_rows, value_rows, cum_gates):
    rows = query_rows.shape[0]
    heads_here = cum_gates.shape[1]
    head_size = query_rows.shape[1] // heads_here
    first_place = lax.axis_index("sp") * rows
    all_gates = gathered_copies(cum_gates, "sp", 0)
    queries = query_rows.reshape(rows, heads_here, head_size)
    query_place = first_place + jnp.arange(rows, dtype=jnp.int32)
    root_scale = head_size ** (-0.5)
    start_state = (
        jnp.full((rows, heads_here), -jnp.inf, jnp.float32),
        jnp.zeros((rows, heads_here), jnp.float32),
        jnp.zeros((rows, heads_here, head_size), jnp.float32),
    )
    key_piece, value_piece = side_by_side((key_rows, value_rows), "sp", 0, 1)
    count = key_piece.shape[0]
    block = math.gcd(count, 512)

    def one_block(number, state):
        top, total, summed = state
        offset = number * block
        key_block = lax.dynamic_slice_in_dim(key_piece, number * block, block, 0).reshape(
            block, heads_here, head_size
        )
        value_block = lax.dynamic_slice_in_dim(value_piece, number * block, block, 0).reshape(
            block, heads_here, head_size
        )
        gate_block = lax.dynamic_slice_in_dim(all_gates, offset, block, 0)
        scores = (
            jnp.einsum("qhd,khd->qhk", queries, key_block, preferred_element_type=jnp.float32)
            * root_scale
        )
        scores = scores + cum_gates[:, :, None] - gate_block.T[None, :, :]
        key_place = offset + jnp.arange(block, dtype=jnp.int32)
        allowed = key_place[None, :] <= query_place[:, None]
        scores = jnp.where(allowed[:, None, :], scores, -jnp.inf)
        new_top = jnp.maximum(top, jnp.max(scores, axis=-1))
        safe_top = jnp.where(new_top == -jnp.inf, 0.0, new_top)
        raised = jnp.exp(scores - safe_top[:, :, None])
        shrink = jnp.exp(top - safe_top)
        total = total * shrink + jnp.sum(raised, axis=-1)
        summed = summed * shrink[:, :, None] + jnp.einsum(
            "qhk,khd->qhd",
            raised.astype(jnp.bfloat16),
            value_block,
            preferred_element_type=jnp.float32,
        )
        return (new_top, total, summed)

    def compute(state):
        return lax.fori_loop(0, count // block, one_block, state)

    def keep_state(state):
        return state

    top, total, summed = lax.cond(
        jnp.int32(0) <= first_place + rows - 1, compute, keep_state, start_state
    )
    return (summed / total[:, :, None]).astype(jnp.bfloat16).reshape(rows, heads_here * head_size)


def body(
    query_rows,
    key_rows,
    value_rows,
    cum_gates,
    residual,
    output_weight,
    norm_gain,
    expert_index,
    route_weights,
    gate_weight,
    up_weight,
    down_weight,
):
    attended = attend_local(query_rows, key_rows, value_rows, cum_gates)
    weight_rows = output_weight
    projected = jnp.dot(
        gathered_copies(attended, "tp", 1), weight_rows, preferred_element_type=jnp.float32
    )
    mixed = (residual.astype(jnp.float32) + projected).astype(jnp.bfloat16)
    rows = residual.shape[0]
    topk = expert_index.shape[1]
    local_experts = gate_weight.shape[0]
    groups = lax.axis_size("sp")
    experts = local_experts * groups
    capacity = 2 * rows * topk // experts
    chosen = expert_index.reshape(rows * topk)
    matches = (chosen[:, None] == jnp.arange(experts, dtype=jnp.int32)[None, :]).astype(jnp.int32)
    rank = jnp.sum((jnp.cumsum(matches, axis=0) - matches) * matches, axis=1)
    slot = chosen * capacity + rank
    owner = jnp.arange(rows * topk, dtype=jnp.int32) // topk
    slot_token = jnp.full((experts * capacity,), rows, jnp.int32).at[slot].set(owner)
    padded = jnp.concatenate([mixed, jnp.zeros((1, mixed.shape[1]), mixed.dtype)], axis=0)
    outgoing = padded[slot_token].reshape(experts, capacity, mixed.shape[1])
    arrived = lax.all_to_all(outgoing, "sp", split_axis=0, concat_axis=0, tiled=True)
    count = arrived.shape[1]
    grouped = arrived.reshape(groups, local_experts, count, arrived.shape[2])
    normed = normalize(lax.all_gather(grouped, "tp", axis=3, tiled=True), norm_gain)
    gate_input = jnp.einsum(
        "seid,edf->seif", normed, gate_weight, preferred_element_type=jnp.float32
    )
    linear_input = jnp.einsum(
        "seid,edf->seif", normed, up_weight, preferred_element_type=jnp.float32
    )
    gate_cut = jnp.minimum(gate_input, CLAMP_LIMIT)
    linear_cut = jnp.clip(linear_input, -CLAMP_LIMIT, CLAMP_LIMIT)
    activated = (gate_cut * jax.nn.sigmoid(SILU_ALPHA * gate_cut) * (linear_cut + 1.0)).astype(
        jnp.bfloat16
    )
    weight_rows = down_weight
    produced = jnp.einsum(
        "seif,efc->seic",
        lax.all_gather(activated, "tp", axis=3, tiled=True),
        weight_rows,
        preferred_element_type=jnp.float32,
    ).astype(jnp.bfloat16)
    returned = lax.all_to_all(
        produced.reshape(groups * local_experts, count, down_weight.shape[2]),
        "sp",
        split_axis=0,
        concat_axis=0,
        tiled=True,
    )
    flat = returned.reshape(experts * capacity, returned.shape[2])
    picked = flat[slot].reshape(rows, topk, flat.shape[1]).astype(jnp.float32)
    blended = jnp.sum(route_weights[:, :, None] * picked, axis=1)
    return (mixed.astype(jnp.float32) + blended).astype(jnp.bfloat16)


def solution(mesh):
    placed = (
        P("sp", "tp"),
        P("sp", "tp"),
        P("sp", "tp"),
        P("sp", "tp"),
        P("sp", "tp"),
        P(None, "tp"),
        P(),
        P("sp", None),
        P("sp", None),
        P("sp", None, "tp"),
        P("sp", None, "tp"),
        P("sp", None, "tp"),
    )
    return jax.shard_map(body, mesh=mesh, in_specs=placed, out_specs=P("sp", "tp"), check_vma=False)
```

profile of v0, /device:TPU:1, one launch (start us, length us, event | category | flops | bytes accessed | tf_op | source)
XLA Modules:
  0.0 568.3 jit_solution(3906957129772426121)
XLA Ops:
  10.7 16.7 %all-to-all-start = ((f32[32,512,1]{1,2,0:T(1,128)}), f32[32,512,1]{1,2,0:T(1,128)S(1)}, u32[]{:S(2)}, u32[]{:S(2)}) async-start(f32[32,512,1]{1,2,0:T(1,128)} %broadcast_in_dim.66), calls=%async_computation | async-start | bytes 131072 | tf_op jit(solution)/shard_map/all_to_all | solution.py:20
  28.4 12.0 %all-to-all-done = f32[32,512,1]{1,2,0:T(1,128)S(1)} async-done(((f32[32,512,1]{1,2,0:T(1,128)}), f32[32,512,1]{1,2,0:T(1,128)S(1)}, u32[]{:S(2)}, u32[]{:S(2)}) %all-to-all-start) | async-done | bytes 65568 | tf_op jit(solution)/shard_map/all_to_all | solution.py:20
  40.4 48.2 %all-gather.5.cloned.1.call-done = bf16[16384,128]{1,0:T(8,128)(2,1)} async-done(((bf16[512,128]{1,0:T(8,128)(2,1)}), bf16[16384,128]{1,0:T(8,128)(2,1)}) %all-gather.5.cloned.1.call-update) | async-done | bytes 4194320 | tf_op jit(solution)/shard_map/all_gather | solution.py:30
  88.6 153.3 %conditional.1 = (f32[512,1]{0,1:T(1,128)}, f32[512,1,64]{0,2,1:T(8,128)}) conditional(s32[]{:T(128)} %convert_element_type.57, () %tuple.27, (bf16[16384,128]{1,0:T(8,128)(2,1)}, f32[32,512,1]{1,2,0:T(1,128)S(1)}, bf16[512,64]{0,1:T(8,128)(2,1)}, s32[]{:T(128)}, s32[512]{0:T(512)S(1)}, /*index=5*/f32[512,1]{0,1:T(1,128)}) %tuple.28), branch_computations={%region_0.0_spmd, %region_1.6_spmd} | conditional | flops 69834240 | bytes 12448155 | solution.py:95
  88.7 7.3 %fusion.71 = (bf16[16384,64]{1,0:T(8,128)(2,1)}, bf16[16384,64]{1,0:T(8,128)(2,1)}) fusion(bf16[16384,128]{1,0:T(8,128)(2,1)} %get-tuple-element.194), kind=kLoop, calls=%fused_computation.85 | loop fusion | bytes 8388608 | tf_op jit(solution)/shard_map/split | solution.py:31
  95.9 145.9 %while.17 = (s32[]{:T(128)}, f32[512,1]{0,1:T(1,128)S(1)}, f32[512,1]{0,1:T(1,128)}, f32[512,1,64]{0,2,1:T(8,128)}, s32[512]{0:T(512)S(1)}, /*index=5*/bf16[1638...) while((s32[]{:T(128)}, f32[512,1]{0,1:T(1,128)S(1)}, ...), condition=%wide.region_5.5_spmd.clone, body=%wide.region_2.4_spmd.clone.sunk | while | flops 69833728 | bytes 3784919 | solution.py:90
  102.5 1.9 fusion.85
  107.1 1.9 fusion.85
  111.7 1.9 fusion.85
  116.3 1.9 fusion.85
  120.9 1.9 fusion.85
  125.4 1.9 fusion.85
  130.0 1.9 fusion.85
  139.2 1.9 fusion.85
  143.8 1.9 fusion.85
  148.3 1.9 fusion.85
  152.9 1.9 fusion.85
  157.5 1.9 fusion.85
  162.1 1.9 fusion.85
  166.7 1.9 fusion.85
  175.8 1.9 fusion.85
  180.4 1.9 fusion.85
  185.0 1.9 fusion.85
  194.1 1.9 fusion.85
  198.7 1.9 fusion.85
  203.3 1.9 fusion.85
  212.4 1.9 fusion.85
  217.0 1.9 fusion.85
  221.6 1.9 fusion.85
  230.8 1.9 fusion.85
  235.3 1.9 fusion.85
  239.9 1.9 fusion.85
  243.9 7.1 %all-to-all-start.1 = ((bf16[16,512,64]{1,2,0:T(8,128)(2,1)}), bf16[16,512,64]{1,2,0:T(8,128)(2,1)S(1)}, u32[]{:S(2)}, u32[]{:S(2)}) async-start(bf16[16,512,64]{1,2,0:T(8,128)(2,1)} %broadcast_in_dim.67), calls=%async_computation.1 | async-start | bytes 2097152 | tf_op jit(solution)/shard_map/all_to_all | solution.py:20
  251.5 9.0 %reduce-window.6 = s32[32,8,128]{2,1,0:T(8,128)S(1)} reduce-window(s32[32,8,128]{2,1,0:T(8,128)S(1)} %fusion.61, s32[]{:T(128)} %constant.103.clone.1), window={size=1x1x128 pad=0_0x0_0x127_0}, to_apply=%region_6.7 | reduce-window | flops 4161536 | bytes 262148 | tf_op jit(solution)/shard_map/reduce-window
  261.1 4.3 scatter_custom_fusion
  265.4 2.0 all-to-all-done.1
  267.9 6.2 %gather_fusion = bf16[2048,128]{1,0:T(8,128)(2,1)S(1)} fusion(bf16[513,128]{1,0:T(8,128)(2,1)S(1)} %concatenate.7, s32[2048]{0:T(1024)S(1)} %fusion.63), kind=kCustom, calls=%fused_computation | custom fusion | bytes 1056768 | tf_op jit(solution)/shard_map/gather | solution.py:134
  274.1 42.7 %all_to_all.20 = bf16[32,64,128]{2,1,0:T(8,128)(2,1)} all-to-all(bf16[32,64,128]{2,1,0:T(8,128)(2,1)S(1)} %bitcast.160), channel_id=1, replica_groups=mesh['sp'=32,'tp'=16] {'sp'}, dimensions={0} | all-to-all | bytes 1048576 | tf_op jit(solution)/shard_map/all_to_all | solution.py:135
  317.1 79.2 %all-gather.9.cloned.1.call-done = bf16[32,64,2048]{2,1,0:T(8,128)(2,1)} async-done(((bf16[32,64,128]{2,1,0:T(8,128)(2,1)}), bf16[32,64,2048]{2,1,0:T(8,128)(2,1)}) %all-gather.9.cloned.1.call-update) | async-done | bytes 8388624 | tf_op jit(solution)/shard_map/all_gather | solution.py:138
  396.3 5.2 fusion.19
  402.0 2.7 fusion.32
  404.7 3.7 fusion.47
  408.5 92.1 %all-gather.7.cloned.1.call-done = bf16[32,1,64,2048]{3,2,0,1:T(8,128)(2,1)} async-done(((bf16[32,1,64,128]{3,2,0,1:T(8,128)(2,1)}), bf16[32,1,64,2048]{3,2,0,1:T(8,128)(2,1)}) %all-gather.7.cloned.1.call-update) | async-done | bytes 8388624 | tf_op jit(solution)/shard_map/all_gather | solution.py:153
  500.6 6.6 %fusion.50 = bf16[32,64,128]{2,1,0:T(8,128)(2,1)} fusion(bf16[32,1,64,2048]{3,2,0,1:T(8,128)(2,1)} %all-gather.7.cloned.1.call-done, bf16[1,2048,128]{2,1,0:T(8,128)(2,1)S(1)} %copy-done.9), kind=kOutput, calls=%fused_computation.49 | convolution fusion | flops 1074003968 | bytes 9437184 | tf_op jit(solution)/shard_map/seif,efc->seic/dot_general | solution.py:151
  507.2 14.4 %all-to-all-start.3 = ((bf16[32,64,128]{2,1,0:T(8,128)(2,1)}), bf16[32,64,128]{2,1,0:T(8,128)(2,1)S(1)}, u32[]{:S(2)}, u32[]{:S(2)}) async-start(bf16[32,64,128]{2,1,0:T(8,128)(2,1)} %fusion.50), calls=%async_computation.3 | async-start | bytes 1048576 | tf_op jit(solution)/shard_map/all_to_all | solution.py:157
  521.7 33.3 %all-to-all-done.3 = bf16[32,64,128]{2,1,0:T(8,128)(2,1)S(1)} async-done(((bf16[32,64,128]{2,1,0:T(8,128)(2,1)}), bf16[32,64,128]{2,1,0:T(8,128)(2,1)S(1)}, u32[]{:S(2)}, u32[]{:S(2)}) %all-to-all-start.3) | async-done | bytes 524320 | tf_op jit(solution)/shard_map/all_to_all | solution.py:157
  555.1 3.2 gather_fusion.1
  558.3 2.8 fusion.54
  (293 shorter events, 105.6 us)
Async XLA Ops:
  6.5 395.0 %copy-start = (bf16[1,2048,128]{2,1,0:T(8,128)(2,1)S(1)}, bf16[1,2048,128]{2,1,0:T(8,128)(2,1)}, u32[]{:S(2)}) copy-start(bf16[1,2048,128]{2,1,0:T(8,128)(2,1)} %param.25) | copy-start | bytes 1572868
  6.5 82.0 %all-gather.5.cloned.1.call-start = ((), (), s32[]{:S(2)}) async-start(), calls=%async_computation.4 | async-start | bytes 4325376 | tf_op jit(solution)/shard_map/all_gather | solution.py:30
  10.7 29.8 %all-to-all-start = ((f32[32,512,1]{1,2,0:T(1,128)}), f32[32,512,1]{1,2,0:T(1,128)S(1)}, u32[]{:S(2)}, u32[]{:S(2)}) async-start(f32[32,512,1]{1,2,0:T(1,128)} %broadcast_in_dim.66), calls=%async_computation | async-start | bytes 131072 | tf_op jit(solution)/shard_map/all_to_all | solution.py:20
  88.6 162.4 %copy-start.4 = (s32[512,2]{0,1:T(2,128)S(1)}, s32[512,2]{0,1:T(2,128)}, u32[]{:S(2)}) copy-start(s32[512,2]{0,1:T(2,128)} %param.23) | copy-start | bytes 12292
  88.6 178.8 %copy-start.2 = (bf16[1024,128]{1,0:T(8,128)(2,1)S(1)}, bf16[1024,128]{1,0:T(8,128)(2,1)}, u32[]{:S(2)}) copy-start(bf16[1024,128]{1,0:T(8,128)(2,1)} %param.21) | copy-start | bytes 786436
  88.6 178.8 %copy-start.3 = (bf16[512,128]{1,0:T(8,128)(2,1)S(1)}, bf16[512,128]{1,0:T(8,128)(2,1)}, u32[]{:S(2)}) copy-start(bf16[512,128]{1,0:T(8,128)(2,1)} %param.20) | copy-start | bytes 393220
  88.6 7.3 %copy-start.7 = (f32[512,1]{0,1:T(1,128)S(1)}, f32[512,1]{0,1:T(1,128)}, u32[]{:S(2)}) copy-start(f32[512,1]{0,1:T(1,128)} %get-tuple-element.359) | copy-start | bytes 6148 | tf_op jit(solution)/shard_map/cond
  88.6 7.3 %copy-start.10 = (bf16[512,64]{0,1:T(8,128)(2,1)S(1)}, bf16[512,64]{0,1:T(8,128)(2,1)}, u32[]{:S(2)}) copy-start(bf16[512,64]{0,1:T(8,128)(2,1)} %get-tuple-element.205) | copy-start | bytes 196612 | tf_op jit(solution)/shard_map/cond
  241.8 75.2 %copy-start.6 = (bf16[2048]{0:T(1024)(128)(2,1)S(1)}, bf16[2048]{0:T(1024)(128)(2,1)}, u32[]{:S(2)}) copy-start(bf16[2048]{0:T(1024)(128)(2,1)} %param.22) | copy-start | bytes 12292
  243.9 23.5 %all-to-all-start.1 = ((bf16[16,512,64]{1,2,0:T(8,128)(2,1)}), bf16[16,512,64]{1,2,0:T(8,128)(2,1)S(1)}, u32[]{:S(2)}, u32[]{:S(2)}) async-start(bf16[16,512,64]{1,2,0:T(8,128)(2,1)} %broadcast_in_dim.67), calls=%async_computation.1 | async-start | bytes 2097152 | tf_op jit(solution)/shard_map/all_to_all | solution.py:20
  250.9 145.3 %all-gather.9.cloned.1.call-start = ((), (), s32[]{:S(2)}) async-start(), calls=%async_computation.6 | async-start | bytes 8912896 | tf_op jit(solution)/shard_map/all_gather | solution.py:138
  316.8 183.8 %all-gather.7.cloned.1.call-start = ((), (), s32[]{:S(2)}) async-start(), calls=%async_computation.5 | async-start | bytes 8912896 | tf_op jit(solution)/shard_map/all_gather | solution.py:153
  396.3 5.8 %copy-start.1 = (bf16[32,64,2048]{2,1,0:T(8,128)(2,1)S(1)}, bf16[32,64,2048]{2,1,0:T(8,128)(2,1)}, u32[]{:S(2)}) copy-start(bf16[32,64,2048]{2,1,0:T(8,128)(2,1)} %all-gather.9.cloned.1.call-done) | copy-start | bytes 25165828
  402.0 2.7 copy-start.8
  404.7 95.9 %copy-start.9 = (bf16[1,2048,128]{2,1,0:T(8,128)(2,1)S(1)}, bf16[1,2048,128]{2,1,0:T(8,128)(2,1)}, u32[]{:S(2)}) copy-start(bf16[1,2048,128]{2,1,0:T(8,128)(2,1)} %param.27) | copy-start | bytes 1572868
  408.5 113.1 %copy-start.5 = (f32[512,2]{0,1:T(2,128)S(1)}, f32[512,2]{0,1:T(2,128)}, u32[]{:S(2)}) copy-start(f32[512,2]{0,1:T(2,128)} %param.24) | copy-start | bytes 12292
  507.2 47.9 %all-to-all-start.3 = ((bf16[32,64,128]{2,1,0:T(8,128)(2,1)}), bf16[32,64,128]{2,1,0:T(8,128)(2,1)S(1)}, u32[]{:S(2)}, u32[]{:S(2)}) async-start(bf16[32,64,128]{2,1,0:T(8,128)(2,1)} %fusion.50), calls=%async_computation.3 | async-start | bytes 1048576 | tf_op jit(solution)/shard_map/all_to_all | solution.py:157
Sparse Core Ops, SparseCore 0:
  9.5 79.0 all-gather.4
  316.9 79.2 all-gather.8
  408.6 91.9 all-gather.6
where the time goes:
time: 571 us; the launch traced here: 568 us
  waiting for transfers between devices  267 us (47%)
  matrix products  115 us (20%)
  other arithmetic  63 us (11%)
  blocking collectives  42.7 us (7%)
  starting transfers between devices  38.5 us (7%)
  local copies, waits for them, and re-layouts  28 us (5%)
  between operations  13.4 us (2%)
    all_gather x1, waiting for transfers between devices, body(): lax.all_gather(activated, 'tp', axis=3, tiled=True)  92.1 us
    all_gather x1, waiting for transfers between devices, body(): lax.all_gather(grouped, 'tp', axis=3, tiled=True)  79.2 us
    dot_general x32, matrix products, one_block(): jnp.einsum('qhk,khd->qhd', raised.astype(jnp.bfloat16), value_block, pref...  61.4 us
    all_gather x1, waiting for transfers between devices, side_by_side(): result = lax.all_gather(both, axis, axis=dim, tiled=True)  48.2 us
    all_to_all x1, blocking collectives, body(): lax.all_to_all(outgoing, 'sp', split_axis=0, concat_axis=0, tiled=True)  42.7 us
    dot_general x32, matrix products, one_block(): jnp.einsum('qhd,khd->qhk', queries, key_block, preferred_element_type=jnp...  40.4 us
    add x32, other arithmetic, one_block(): total = total * shrink + jnp.sum(raised, axis=-1)  36.7 us
    all_to_all x1, waiting for transfers between devices, body(): lax.all_to_all(produced.reshape(groups * local_experts, count, down_weigh...  33.3 us
  transfers between devices with their start and end apart: 6, of which 6 were waited for; matrix products, arithmetic and copies ran while one was open for 3% of the time, Pallas kernels for 0%

commit v1 on v0

--- a/solution.py
+++ b/solution.py
@@ -150,7 +150,9 @@
     weight_rows = down_weight
     produced = jnp.einsum(
         "seif,efc->seic",
-        lax.all_gather(activated, "tp", axis=3, tiled=True),
+        jnp.concatenate(
+            lax.all_to_all(jnp.stack([activated] * lax.axis_size("tp")), "tp", 0, 0), axis=3
+        ),
         weight_rows,
         preferred_element_type=jnp.float32,
     ).astype(jnp.bfloat16)

time: 571 us -> 623 us (1.091)
  blocking collectives: 42.7 us -> 143 us
  waiting for transfers between devices: 267 us -> 175 us
  local copies, waits for them, and re-layouts: 28 us -> 66.7 us
    all_to_all x0 -> x1, blocking collectives: none -> 100 us  [body(): lax.all_to_all(jnp.stack([activated] * lax.axis_size('tp')), 'tp', 0, 0)]
    all_gather x1 -> x0, waiting for transfers between devices: 92.1 us -> none  [body(): lax.all_gather(activated, 'tp', axis=3, tiled=True)]
    reshape x0 -> x1, local copies, waits for them, and re-layouts: none -> 23.1 us  [body(): jnp.concatenate(lax.all_to_all(jnp.stack([activated] * lax.axis_size('tp'...]
    another operation x2 -> x4, local copies, waits for them, and re-layouts: 0.08 us -> 15.6 us
  transfers between devices with their start and end apart: 6 -> 5, of which waited for: 6 -> 5; matrix products, arithmetic and copies ran while one was open for 3% -> 3% of each run, Pallas kernels for 0% -> 0%
where the time goes in v1:
time: 623 us; the launch traced here: 620 us
  waiting for transfers between devices  175 us (28%)
  blocking collectives  143 us (23%)
  matrix products  115 us (18%)
  other arithmetic  67.1 us (11%)
  local copies, waits for them, and re-layouts  66.7 us (11%)
  starting transfers between devices  39.4 us (6%)
  between operations  13.7 us (2%)
    all_to_all x1, blocking collectives, body(): lax.all_to_all(jnp.stack([activated] * lax.axis_size('tp')), 'tp', 0, 0)  100 us
    all_gather x1, waiting for transfers between devices, body(): lax.all_gather(grouped, 'tp', axis=3, tiled=True)  79.4 us
    dot_general x32, matrix products, one_block(): jnp.einsum('qhk,khd->qhd', raised.astype(jnp.bfloat16), value_block, pref...  61.5 us
    all_gather x1, waiting for transfers between devices, side_by_side(): result = lax.all_gather(both, axis, axis=dim, tiled=True)  48.2 us
    all_to_all x1, blocking collectives, body(): lax.all_to_all(outgoing, 'sp', split_axis=0, concat_axis=0, tiled=True)  42.7 us
    add x32, other arithmetic, one_block(): total = total * shrink + jnp.sum(raised, axis=-1)  40.8 us
    dot_general x32, matrix products, one_block(): jnp.einsum('qhd,khd->qhk', queries, key_block, preferred_element_type=jnp...  40.8 us
    all_to_all x1, waiting for transfers between devices, body(): lax.all_to_all(produced.reshape(groups * local_experts, count, down_weigh...  33.3 us
  transfers between devices with their start and end apart: 5, of which 5 were waited for; matrix products, arithmetic and copies ran while one was open for 3% of the time, Pallas kernels for 0%

profile of v1, /device:TPU:1, one launch (start us, length us, event | category | flops | bytes accessed | tf_op | source)
XLA Modules:
  0.0 620.0 jit_solution(5338646229577842446)
XLA Ops:
  10.7 16.7 %all-to-all-start = ((f32[32,512,1]{1,2,0:T(1,128)}), f32[32,512,1]{1,2,0:T(1,128)S(1)}, u32[]{:S(2)}, u32[]{:S(2)}) async-start(f32[32,512,1]{1,2,0:T(1,128)} %broadcast_in_dim.66), calls=%async_computation | async-start | bytes 131072 | tf_op jit(solution)/shard_map/all_to_all | solution.py:20
  28.4 12.0 %all-to-all-done = f32[32,512,1]{1,2,0:T(1,128)S(1)} async-done(((f32[32,512,1]{1,2,0:T(1,128)}), f32[32,512,1]{1,2,0:T(1,128)S(1)}, u32[]{:S(2)}, u32[]{:S(2)}) %all-to-all-start) | async-done | bytes 65568 | tf_op jit(solution)/shard_map/all_to_all | solution.py:20
  40.4 48.2 %all-gather.4.cloned.1.call-done = bf16[16384,128]{1,0:T(8,128)(2,1)} async-done(((bf16[512,128]{1,0:T(8,128)(2,1)}), bf16[16384,128]{1,0:T(8,128)(2,1)}) %all-gather.4.cloned.1.call-update) | async-done | bytes 4194320 | tf_op jit(solution)/shard_map/all_gather | solution.py:30
  88.6 157.9 %conditional.1 = (f32[512,1]{0,1:T(1,128)}, f32[512,1,64]{0,2,1:T(8,128)}) conditional(s32[]{:T(128)} %convert_element_type.59, () %tuple.27, (bf16[16384,128]{1,0:T(8,128)(2,1)}, f32[32,512,1]{1,2,0:T(1,128)S(1)}, bf16[512,64]{0,1:T(8,128)(2,1)}, s32[]{:T(128)}, s32[512]{0:T(512)S(1)}, /*index=5*/f32[512,1]{0,1:T(1,128)}) %tuple.28), branch_computations={%region_0.0_spmd, %region_1.6_spmd} | conditional | flops 69834240 | bytes 12448147 | solution.py:95
  88.6 7.3 %fusion.69 = (bf16[16384,64]{1,0:T(8,128)(2,1)}, bf16[16384,64]{1,0:T(8,128)(2,1)}) fusion(bf16[16384,128]{1,0:T(8,128)(2,1)} %get-tuple-element.194), kind=kLoop, calls=%fused_computation.84 | loop fusion | bytes 8388608 | tf_op jit(solution)/shard_map/split | solution.py:31
  96.0 150.5 %while.17 = (s32[]{:T(128)}, f32[512,1]{0,1:T(1,128)S(1)}, f32[512,1]{0,1:T(1,128)}, f32[512,1,64]{0,2,1:T(8,128)}, s32[512]{0:T(512)S(1)}, /*index=5*/bf16[1638...) while((s32[]{:T(128)}, f32[512,1]{0,1:T(1,128)S(1)}, ...), condition=%wide.region_5.5_spmd.clone, body=%wide.region_2.4_spmd.clone.sunk | while | flops 69833728 | bytes 3784911 | solution.py:90
  102.8 1.9 fusion.84
  107.5 1.9 fusion.84
  112.2 1.9 fusion.84
  117.0 1.9 fusion.84
  121.7 1.9 fusion.84
  126.4 1.9 fusion.84
  131.1 1.9 fusion.84
  135.9 1.9 fusion.84
  140.6 1.9 fusion.84
  145.3 1.9 fusion.84
  150.0 1.9 fusion.84
  154.8 1.9 fusion.84
  159.5 1.9 fusion.84
  168.9 1.9 fusion.84
  178.4 1.9 fusion.84
  187.8 1.9 fusion.84
  197.3 1.9 fusion.84
  206.7 1.9 fusion.84
  216.2 1.9 fusion.84
  220.9 1.9 fusion.84
  225.6 1.9 fusion.84
  230.3 1.9 fusion.84
  239.8 1.9 fusion.84
  248.5 7.1 %all-to-all-start.1 = ((bf16[16,512,64]{1,2,0:T(8,128)(2,1)}), bf16[16,512,64]{1,2,0:T(8,128)(2,1)S(1)}, u32[]{:S(2)}, u32[]{:S(2)}) async-start(bf16[16,512,64]{1,2,0:T(8,128)(2,1)} %broadcast_in_dim.67), calls=%async_computation.1 | async-start | bytes 2097152 | tf_op jit(solution)/shard_map/all_to_all | solution.py:20
  255.8 9.0 %reduce-window.6 = s32[32,8,128]{2,1,0:T(8,128)S(1)} reduce-window(s32[32,8,128]{2,1,0:T(8,128)S(1)} %fusion.59, s32[]{:T(128)} %constant.103.clone.1), window={size=1x1x128 pad=0_0x0_0x127_0}, to_apply=%region_6.7 | reduce-window | flops 4161536 | bytes 262148 | tf_op jit(solution)/shard_map/reduce-window
  265.7 4.3 scatter_custom_fusion
  270.0 2.0 all-to-all-done.1
  272.5 6.2 gather_fusion
  278.7 42.7 %all_to_all.25 = bf16[32,64,128]{2,1,0:T(8,128)(2,1)} all-to-all(bf16[32,64,128]{2,1,0:T(8,128)(2,1)S(1)} %bitcast.170), channel_id=1, replica_groups=mesh['sp'=32,'tp'=16] {'sp'}, dimensions={0} | all-to-all | bytes 1048576 | tf_op jit(solution)/shard_map/all_to_all | solution.py:135
  321.4 79.4 %all-gather.6.cloned.1.call-done = bf16[32,64,2048]{2,1,0:T(8,128)(2,1)} async-done(((bf16[32,64,128]{2,1,0:T(8,128)(2,1)}), bf16[32,64,2048]{2,1,0:T(8,128)(2,1)}) %all-gather.6.cloned.1.call-update) | async-done | bytes 8388624 | tf_op jit(solution)/shard_map/all_gather | solution.py:138
  400.8 5.2 fusion.19
  406.6 2.7 fusion.30
  409.3 2.9 fusion.48
  412.2 2.1 stack.2
  414.4 100.0 %all_to_all.26 = bf16[16,32,1,64,128]{4,3,1,2,0:T(8,128)(2,1)} all-to-all(bf16[16,32,1,64,128]{4,3,1,2,0:T(8,128)(2,1)S(1)} %stack.2), channel_id=1, replica_groups=mesh['sp'=32,'tp'=16] {'tp'}, dimensions={0} | all-to-all | bytes 16777216 | tf_op jit(solution)/shard_map/all_to_all | solution.py:154
  514.4 23.1 %copy.36 = bf16[32,1,64,16,128]{4,3,2,0,1:T(8,128)(2,1)} copy(bf16[32,1,64,16,128]{4,2,0,1,3:T(8,128)(2,1)} %bitcast.167) | data formatting | bytes 16777216 | tf_op jit(solution)/shard_map/reshape | solution.py:153
  537.5 13.4 %reshape.237 = bf16[32,64,2048]{2,1,0:T(8,128)(2,1)} reshape(bf16[32,1,64,16,128]{4,3,2,0,1:T(8,128)(2,1)} %copy.36) | data formatting | bytes 16777216 | tf_op jit(solution)/shard_map/reshape.33
  550.9 6.5 %convolution_convert_fusion = bf16[32,64,128]{2,1,0:T(8,128)(2,1)} fusion(bf16[32,64,2048]{2,1,0:T(8,128)(2,1)} %reshape.237, bf16[1,2048,128]{2,1,0:T(8,128)(2,1)S(1)} %copy-done.9), kind=kOutput, calls=%fused_computation.47 | convolution fusion | flops 1074003968 | bytes 9437184 | tf_op jit(solution)/shard_map/seif,efc->seic/dot_general | solution.py:151
  557.4 15.5 %all-to-all-start.4 = ((bf16[32,64,128]{2,1,0:T(8,128)(2,1)}), bf16[32,64,128]{2,1,0:T(8,128)(2,1)S(1)}, u32[]{:S(2)}, u32[]{:S(2)}) async-start(bf16[32,64,128]{2,1,0:T(8,128)(2,1)} %convolution_convert_fusion), calls=%async_computation.4 | async-start | bytes 1048576 | tf_op jit(solution)/shard_map/all_to_all | solution.py:159
  573.1 33.3 %all-to-all-done.4 = bf16[32,64,128]{2,1,0:T(8,128)(2,1)S(1)} async-done(((bf16[32,64,128]{2,1,0:T(8,128)(2,1)}), bf16[32,64,128]{2,1,0:T(8,128)(2,1)S(1)}, u32[]{:S(2)}, u32[]{:S(2)}) %all-to-all-start.4) | async-done | bytes 524320 | tf_op jit(solution)/shard_map/all_to_all | solution.py:159
  606.4 3.2 gather_fusion.1
  609.6 2.8 fusion.52
  (294 shorter events, 115.6 us)
Async XLA Ops:
  6.5 399.5 %copy-start = (bf16[1,2048,128]{2,1,0:T(8,128)(2,1)S(1)}, bf16[1,2048,128]{2,1,0:T(8,128)(2,1)}, u32[]{:S(2)}) copy-start(bf16[1,2048,128]{2,1,0:T(8,128)(2,1)} %param.25) | copy-start | bytes 1572868
  6.5 82.0 %all-gather.4.cloned.1.call-start = ((), (), s32[]{:S(2)}) async-start(), calls=%async_computation.5 | async-start | bytes 4325376 | tf_op jit(solution)/shard_map/all_gather | solution.py:30
  10.7 29.8 %all-to-all-start = ((f32[32,512,1]{1,2,0:T(1,128)}), f32[32,512,1]{1,2,0:T(1,128)S(1)}, u32[]{:S(2)}, u32[]{:S(2)}) async-start(f32[32,512,1]{1,2,0:T(1,128)} %broadcast_in_dim.66), calls=%async_computation | async-start | bytes 131072 | tf_op jit(solution)/shard_map/all_to_all | solution.py:20
  88.6 167.0 %copy-start.4 = (s32[512,2]{0,1:T(2,128)S(1)}, s32[512,2]{0,1:T(2,128)}, u32[]{:S(2)}) copy-start(s32[512,2]{0,1:T(2,128)} %param.23) | copy-start | bytes 12292
  88.6 183.4 %copy-start.2 = (bf16[1024,128]{1,0:T(8,128)(2,1)S(1)}, bf16[1024,128]{1,0:T(8,128)(2,1)}, u32[]{:S(2)}) copy-start(bf16[1024,128]{1,0:T(8,128)(2,1)} %param.21) | copy-start | bytes 786436
  88.6 183.4 %copy-start.3 = (bf16[512,128]{1,0:T(8,128)(2,1)S(1)}, bf16[512,128]{1,0:T(8,128)(2,1)}, u32[]{:S(2)}) copy-start(bf16[512,128]{1,0:T(8,128)(2,1)} %param.20) | copy-start | bytes 393220
  88.6 7.4 %copy-start.7 = (f32[512,1]{0,1:T(1,128)S(1)}, f32[512,1]{0,1:T(1,128)}, u32[]{:S(2)}) copy-start(f32[512,1]{0,1:T(1,128)} %get-tuple-element.359) | copy-start | bytes 6148 | tf_op jit(solution)/shard_map/cond
  88.6 7.4 %copy-start.10 = (bf16[512,64]{0,1:T(8,128)(2,1)S(1)}, bf16[512,64]{0,1:T(8,128)(2,1)}, u32[]{:S(2)}) copy-start(bf16[512,64]{0,1:T(8,128)(2,1)} %get-tuple-element.205) | copy-start | bytes 196612 | tf_op jit(solution)/shard_map/cond
  246.4 75.0 %copy-start.6 = (bf16[2048]{0:T(1024)(128)(2,1)S(1)}, bf16[2048]{0:T(1024)(128)(2,1)}, u32[]{:S(2)}) copy-start(bf16[2048]{0:T(1024)(128)(2,1)} %param.22) | copy-start | bytes 12292
  248.5 23.5 %all-to-all-start.1 = ((bf16[16,512,64]{1,2,0:T(8,128)(2,1)}), bf16[16,512,64]{1,2,0:T(8,128)(2,1)S(1)}, u32[]{:S(2)}, u32[]{:S(2)}) async-start(bf16[16,512,64]{1,2,0:T(8,128)(2,1)} %broadcast_in_dim.67), calls=%async_computation.1 | async-start | bytes 2097152 | tf_op jit(solution)/shard_map/all_to_all | solution.py:20
  255.5 145.3 %all-gather.6.cloned.1.call-start = ((), (), s32[]{:S(2)}) async-start(), calls=%async_computation.6 | async-start | bytes 8912896 | tf_op jit(solution)/shard_map/all_gather | solution.py:138
  400.8 5.8 copy-start.1
  406.6 2.7 copy-start.8
  537.5 13.4 %copy-start.9 = (bf16[1,2048,128]{2,1,0:T(8,128)(2,1)S(1)}, bf16[1,2048,128]{2,1,0:T(8,128)(2,1)}, u32[]{:S(2)}) copy-start(bf16[1,2048,128]{2,1,0:T(8,128)(2,1)} %param.27) | copy-start | bytes 1572868
  550.9 22.0 %copy-start.5 = (f32[512,2]{0,1:T(2,128)S(1)}, f32[512,2]{0,1:T(2,128)}, u32[]{:S(2)}) copy-start(f32[512,2]{0,1:T(2,128)} %param.24) | copy-start | bytes 12292
  557.4 49.0 %all-to-all-start.4 = ((bf16[32,64,128]{2,1,0:T(8,128)(2,1)}), bf16[32,64,128]{2,1,0:T(8,128)(2,1)S(1)}, u32[]{:S(2)}, u32[]{:S(2)}) async-start(bf16[32,64,128]{2,1,0:T(8,128)(2,1)} %convolution_convert_fusion), calls=%async_computation.4 | async-start | bytes 1048576 | tf_op jit(solution)/shard_map/all_to_all | solution.py:159
Sparse Core Ops, SparseCore 0:
  9.5 79.0 all-gather.3
  321.5 79.2 all-gather.5
